TPU v7x, 32 devices: a whole 2x2x4 slice. The times are simulated.
32 devices in a mesh: sp: 8 (over z, x), dp: 4 (over y, core).
Axes of the slice: x: 2, y: 2, z: 4, core: 2. Of those that a mesh axis runs over, the one named last changes fastest.
Arguments:
- inputs: bfloat16 [1536, 2048], P('sp'), may hold values from -6 to 6
- w_query: bfloat16 [2048, 2048], P('dp'), may hold values from -0.125 to 0.125
- w_key: bfloat16 [1024, 2048], P('dp'), may hold values from -0.125 to 0.125
- w_value: bfloat16 [1024, 2048], P('dp'), may hold values from -0.125 to 0.125
- query_gain: float32 [64], replicated, may hold values from 0.6 to 7
- key_gain: float32 [64], replicated, may hold values from 0.6 to 7
- grad_out: bfloat16 [1536, 2048], P('sp', 'dp'), may hold values from -6 to 6
Outputs:
- d_inputs: bfloat16 [1536, 2048], P('sp', 'dp')
- grad_wq: float32 [2048, 2048], P('dp')
- grad_wk: float32 [1024, 2048], P('dp')
- grad_wv: float32 [1024, 2048], P('dp')
All inputs are finite; a program needn't handle non-finite values.
Results may differ from a plain program's by a relative error of at most 0.019.
The roundings to bfloat16 on the way count: a program that leaves them out, or rounds other values in their place, can miss the bound.
Values may be sent and summed in bfloat16 or wider, within the bound.
No kernel may reach another device: no remote copies, remote signals or barrier semaphores. Data moves between devices by JAX's collectives and lax.ppermute only.
A program may use at most 64 MiB of HBM per device.

v0:
```python
import jax
import jax.numpy as jnp
from jax import lax
from jax.sharding import PartitionSpec as P

HEAD_WIDTH = 64
GRID_W = 64
norm_eps = 1e-06
axial_base = 10000.0


def rotation_tables(offset, count):
    positions = offset + jnp.arange(count, dtype=jnp.int32)
    grid_rows = (positions // GRID_W).astype(jnp.float32)
    grid_cols = (positions % GRID_W).astype(jnp.float32)
    quarter = HEAD_WIDTH // 4
    freqs_axis = axial_base ** (-jnp.arange(quarter, dtype=jnp.float32) / quarter)
    angle_rows = grid_rows[:, None] * freqs_axis[None, :]
    angle_cols = grid_cols[:, None] * freqs_axis[None, :]
    cosine = jnp.concatenate(
        [jnp.cos(angle_rows), jnp.cos(angle_rows), jnp.cos(angle_cols), jnp.cos(angle_cols)], axis=1
    )
    sine = jnp.concatenate(
        [jnp.sin(angle_rows), jnp.sin(angle_rows), jnp.sin(angle_cols), jnp.sin(angle_cols)], axis=1
    )
    return (cosine, sine)


def quarter_turn(values):
    quarter = HEAD_WIDTH // 4
    return jnp.concatenate(
        [
            -values[..., quarter : 2 * quarter],
            values[..., :quarter],
            -values[..., 3 * quarter :],
            values[..., 2 * quarter : 3 * quarter],
        ],
        axis=-1,
    )


def quarter_back(values):
    quarter = HEAD_WIDTH // 4
    return jnp.concatenate(
        [
            values[..., quarter : 2 * quarter],
            -values[..., :quarter],
            values[..., 3 * quarter :],
            -values[..., 2 * quarter : 3 * quarter],
        ],
        axis=-1,
    )


def rotate(values, cosine, sine):
    return values * cosine + quarter_turn(values) * sine


def rotate_back(grads, cosine, sine):
    return grads * cosine + quarter_back(grads * sine)


def head_norm(raw):
    scale_inv = lax.rsqrt(jnp.mean(raw * raw, axis=-1, keepdims=True) + norm_eps)
    return (raw * scale_inv, scale_inv)


def head_norm_back(grads, normed, scale_inv, gain):
    scaled = grads * gain
    return scale_inv * (scaled - normed * jnp.mean(scaled * normed, axis=-1, keepdims=True))


def body(inputs, w_query, w_key, w_value, query_gain, key_gain, grad_out):
    tok_rows = inputs.shape[0]
    local_query = w_query.shape[0] // HEAD_WIDTH
    local_keys = w_key.shape[0] // HEAD_WIDTH
    group = local_query // local_keys
    key_width = local_keys * HEAD_WIDTH
    scale = HEAD_WIDTH ** (-0.5)
    contract = (((1,), (1,)), ((), ()))
    leading = (((0,), (0,)), ((), ()))
    offset = lax.axis_index("sp") * tok_rows
    cosine, sine = rotation_tables(offset, tok_rows)
    cos_wide = cosine[:, None, :]
    sin_wide = sine[:, None, :]
    q_raw = lax.dot_general(inputs, w_query, contract, preferred_element_type=jnp.float32).astype(
        jnp.bfloat16
    )
    w_pair = jnp.concatenate([w_key, w_value], axis=0)
    kv_raw = lax.dot_general(inputs, w_pair, contract, preferred_element_type=jnp.float32).astype(
        jnp.bfloat16
    )
    q_wide = (
        lax.optimization_barrier(q_raw)
        .astype(jnp.float32)
        .reshape(tok_rows, local_query, HEAD_WIDTH)
    )
    k_wide = (
        lax.optimization_barrier(kv_raw[:, :key_width])
        .astype(jnp.float32)
        .reshape(tok_rows, local_keys, HEAD_WIDTH)
    )
    q_normed, q_inv = head_norm(q_wide)
    k_normed, k_inv = head_norm(k_wide)
    q_rot = rotate(q_normed * query_gain, cos_wide, sin_wide).astype(jnp.bfloat16)
    k_rot = rotate(k_normed * key_gain, cos_wide, sin_wide).astype(jnp.bfloat16)
    kv_rot = jnp.concatenate([k_rot.reshape(tok_rows, key_width), kv_raw[:, key_width:]], axis=1)
    kv_every = lax.all_gather(kv_rot, "sp", axis=0, tiled=True)
    seq_rows = kv_every.shape[0]
    keys_every = kv_every[:, :key_width]
    values_every = kv_every[:, key_width:]
    grad_query = []
    log_totals = []
    deltas = []
    key_terms = [jnp.zeros((seq_rows, HEAD_WIDTH), jnp.float32) for slot in range(local_keys)]
    value_terms = [jnp.zeros((seq_rows, HEAD_WIDTH), jnp.float32) for slot in range(local_keys)]
    for member in range(local_query):
        kv_index = member // group
        query_head = q_rot[:, member, :]
        key_head = keys_every[:, kv_index * HEAD_WIDTH : (kv_index + 1) * HEAD_WIDTH]
        value_head = values_every[:, kv_index * HEAD_WIDTH : (kv_index + 1) * HEAD_WIDTH]
        grad_head = grad_out[:, member * HEAD_WIDTH : (member + 1) * HEAD_WIDTH]
        scores = (
            lax.dot_general(query_head, key_head, contract, preferred_element_type=jnp.float32)
            * scale
        )
        maxima = jnp.max(scores, axis=1, keepdims=True)
        log_total = maxima + jnp.log(jnp.sum(jnp.exp(scores - maxima), axis=1, keepdims=True))
        prob_exact = jnp.exp(scores - log_total)
        prob_half = prob_exact.astype(jnp.bfloat16)
        attn_rows = jnp.dot(prob_half, value_head, preferred_element_type=jnp.float32).astype(
            jnp.bfloat16
        )
        attn_wide = lax.optimization_barrier(attn_rows).astype(jnp.float32)
        delta_rows = jnp.sum(grad_head.astype(jnp.float32) * attn_wide, axis=1, keepdims=True)
        dprob = lax.dot_general(grad_head, value_head, contract, preferred_element_type=jnp.float32)
        dscore = (prob_exact * (dprob - delta_rows)).astype(jnp.bfloat16)
        grad_query.append(jnp.dot(dscore, key_head, preferred_element_type=jnp.float32) * scale)
        log_totals.append(log_total)
        deltas.append(delta_rows)
        value_terms[kv_index] = value_terms[kv_index] + lax.dot_general(
            prob_half, grad_head, leading, preferred_element_type=jnp.float32
        )
        key_terms[kv_index] = (
            key_terms[kv_index]
            + lax.dot_general(dscore, query_head, leading, preferred_element_type=jnp.float32)
            * scale
        )
    gradient_query_rotated = jnp.stack(grad_query, axis=1)
    partial_sums = jnp.concatenate(key_terms + value_terms, axis=1)
    own_grads = lax.psum_scatter(partial_sums, "sp", scatter_dimension=0, tiled=True)
    gradient_key_rotated = own_grads[:, :key_width].reshape(tok_rows, local_keys, HEAD_WIDTH)
    grad_q = head_norm_back(
        rotate_back(gradient_query_rotated, cos_wide, sin_wide), q_normed, q_inv, query_gain
    )
    grad_q = grad_q.reshape(tok_rows, local_query * HEAD_WIDTH).astype(jnp.bfloat16)
    grad_k = head_norm_back(
        rotate_back(gradient_key_rotated, cos_wide, sin_wide), k_normed, k_inv, key_gain
    )
    grad_kv = jnp.concatenate(
        [
            grad_k.reshape(tok_rows, key_width).astype(jnp.bfloat16),
            own_grads[:, key_width:].astype(jnp.bfloat16),
        ],
        axis=1,
    )
    head_part = jnp.dot(grad_q, w_query, preferred_element_type=jnp.float32)
    head_part = head_part + jnp.dot(grad_kv, w_pair, preferred_element_type=jnp.float32)
    d_inputs = lax.psum_scatter(
        head_part.astype(jnp.bfloat16), "dp", scatter_dimension=1, tiled=True
    )
    grad_wq = lax.dot_general(grad_q, inputs, leading, preferred_element_type=jnp.float32)
    grad_wkv = lax.dot_general(grad_kv, inputs, leading, preferred_element_type=jnp.float32)
    grad_wq, grad_wkv = lax.psum((grad_wq, grad_wkv), "sp")
    return (d_inputs, grad_wq, grad_wkv[:key_width], grad_wkv[key_width:])


def solution(mesh):
    return jax.shard_map(
        body,
        mesh=mesh,
        in_specs=(
            P("sp", None),
            P("dp", None),
            P("dp", None),
            P("dp", None),
            P(),
            P(),
            P("sp", "dp"),
        ),
        out_specs=(P("sp", "dp"), P("dp", None), P("dp", None), P("dp", None)),
        check_vma=False,
    )
```

profile of v0, /device:TPU:0, one launch (start us, length us, event | category | flops | bytes accessed | tf_op | source)
XLA Modules:
  0.0 498.9 jit_solution(4581374337283304342)
XLA Ops:
  9.1 1.4 constant_dynamic-update-slice_fusion.1
  16.6 1.7 copy.97
  21.3 1.6 pad_maximum_fusion.1
  22.9 1.5 convolution_convert_fusion.1
  25.2 1.5 copy.126
  26.7 1.5 copy.125
  34.6 35.3 %all-gather.2.cloned.1.call-done = bf16[1536,512]{1,0:T(8,128)(2,1)} async-done(((bf16[192,512]{1,0:T(8,128)(2,1)}), bf16[1536,512]{1,0:T(8,128)(2,1)}) %all-gather.2.cloned.1.call-update) | async-done | bytes 1572880 | tf_op jit(solution)/shard_map/all_gather | solution.py:108
  69.9 1.6 fusion.148
  95.9 1.1 fusion.28
  97.1 1.1 fusion.27
  100.5 3.5 copy.117
  106.2 2.0 copy.109
  108.3 1.6 fusion.53
  109.9 1.6 fusion.51
  111.5 1.7 fusion.49
  116.6 1.6 multiply_reduce_fusion
  118.2 2.0 copy.106
  121.8 1.4 multiply_convert_fusion
  123.2 2.8 fusion.156
  126.0 51.0 %reduce-scatter.7.cloned.1.call-done = f32[192,512]{1,0:T(8,128)} async-done(((f32[1536,512]{1,0:T(8,128)}), f32[192,512]{1,0:T(8,128)}) %reduce-scatter.7.cloned.1.call-update) | async-done | bytes 393232 | tf_op jit(solution)/shard_map/reduce_scatter | solution.py:151
  177.0 1.6 slice.233
  178.6 1.8 copy.112
  181.5 1.6 pad_maximum_fusion
  183.1 1.8 copy.113
  185.7 1.7 copy.114
  188.4 1.3 multiply_convert_fusion.1
  190.3 2.7 fusion.96
  194.8 1.5 fusion.16
  196.3 266.0 %all-reduce.3.cloned.1.call-done = (f32[512,2048]{1,0:T(8,128)}, f32[512,2048]{1,0:T(8,128)}) async-done(((f32[512,2048]{1,0:T(8,128)}, f32[512,2048]{1,0:T(8,128)}), (f32[512,2048]{1,0:T(8,128)}, f32[512,2048]{1,0:T(8,128)})) %all-reduce.3.cloned.1.call-update) | async-done | bytes 8388624 | tf_op jit(solution)/shard_map/psum | solution.py:174
  462.3 4.7 fusion.142
  467.0 20.6 %reduce-scatter.5.cloned.1.call-done = bf16[192,512]{1,0:T(8,128)(2,1)} async-done(((bf16[192,2048]{1,0:T(8,128)(2,1)}), bf16[192,512]{1,0:T(8,128)(2,1)}) %reduce-scatter.5.cloned.1.call-update) | async-done | bytes 196624 | tf_op jit(solution)/shard_map/reduce_scatter | solution.py:169
  487.7 4.7 copy.144
  (222 shorter events, 56.7 us)
Async XLA Ops:
  7.2 15.8 %copy-start = (bf16[512,2048]{1,0:T(8,128)(2,1)S(1)}, bf16[512,2048]{1,0:T(8,128)(2,1)}, u32[]{:S(2)}) copy-start(bf16[512,2048]{1,0:T(8,128)(2,1)} %param.8) | copy-start | bytes 6291460
  7.2 62.7 %all-gather.2.cloned.1.call-start = ((), (), s32[]{:S(2)}) async-start(), calls=%async_computation.2 | async-start | bytes 1769472 | tf_op jit(solution)/shard_map/all_gather | solution.py:108
  8.1 12.0 %copy-start.43 = (f32[256]{0:T(256)}, f32[256]{0:T(256)S(1)}, u32[]{:S(2)}) copy-start(f32[256]{0:T(256)S(1)} %mul.354) | copy-start | bytes 3076
  9.0 107.1 %copy-start.29 = (f32[192,64]{0,1:T(8,128)}, f32[192,64]{0,1:T(8,128)S(1)}, u32[]{:S(2)}) copy-start(f32[192,64]{0,1:T(8,128)S(1)} %pad_maximum_fusion.5) | copy-start | bytes 147460
  9.1 11.0 %copy-start.25 = (f32[192,256]{1,0:T(8,128)}, f32[192,256]{1,0:T(8,128)S(1)}, u32[]{:S(2)}) copy-start(f32[192,256]{1,0:T(8,128)S(1)} %copy.96) | copy-start | bytes 589828
  9.1 1.6 copy-start.30
  10.7 1.1 copy-start.3
  11.9 1.3 copy-start.19
  11.9 3.1 copy-start.48
  14.9 3.5 copy-start.21
  20.1 2.7 copy-start.27
  22.9 1.6 copy-start.4
  22.9 154.1 %reduce-scatter.7.cloned.1.call-start = ((), (), s32[]{:S(2)}) async-start(), calls=%async_computation.4 | async-start | bytes 3538944 | tf_op jit(solution)/shard_map/reduce_scatter | solution.py:151
  24.5 9.1 %copy-start.45 = (f32[64]{0:T(128)S(1)}, f32[64]{0:T(128)}, u32[]{:S(2)}) copy-start(f32[64]{0:T(128)} %param.11) | copy-start | bytes 772
  69.9 1.9 copy-start.1
  94.9 2.1 copy-start.12
  104.0 358.3 %all-reduce.3.cloned.1.call-start = ((), (), s32[]{:S(2)}) async-start(), calls=%async_computation.5 | async-start | bytes 16777216 | tf_op jit(solution)/shard_map/psum | solution.py:174
  108.3 3.2 copy-start.2
  109.9 3.3 copy-start.17
  111.5 2.2 copy-start.9
  113.7 1.1 copy-start.7
  114.2 1.1 copy-start.13
  118.1 3.7 copy-start.47
  126.0 55.5 %copy-start.22 = (f32[192,256]{0,1:T(8,128)S(1)}, f32[192,256]{0,1:T(8,128)}, u32[]{:S(2)}) copy-start(f32[192,256]{0,1:T(8,128)} %copy-done.21) | copy-start | bytes 589828
  126.0 55.5 %copy-start.49 = (f32[64]{0:T(128)S(1)}, f32[64]{0:T(128)}, u32[]{:S(2)}) copy-start(f32[64]{0:T(128)} %param.12) | copy-start | bytes 772
  180.4 1.1 copy-start.24
  181.5 6.8 %copy-start.26 = (f32[192,256]{1,0:T(8,128)S(1)}, f32[192,256]{1,0:T(8,128)}, u32[]{:S(2)}) copy-start(f32[192,256]{1,0:T(8,128)} %copy-done.25) | copy-start | bytes 589828
  181.5 6.8 %copy-start.44 = (f32[256]{0:T(256)S(1)}, f32[256]{0:T(256)}, u32[]{:S(2)}) copy-start(f32[256]{0:T(256)} %copy-done.43) | copy-start | bytes 3076
  183.1 5.2 %copy-start.28 = (f32[192,256]{1,0:T(8,128)S(1)}, f32[192,256]{1,0:T(8,128)}, u32[]{:S(2)}) copy-start(f32[192,256]{1,0:T(8,128)} %copy-done.27) | copy-start | bytes 589828
  188.4 1.3 copy-start.31
  193.1 294.6 %reduce-scatter.5.cloned.1.call-start = ((), (), s32[]{:S(2)}) async-start(), calls=%async_computation.3 | async-start | bytes 983040 | tf_op jit(solution)/shard_map/reduce_scatter | solution.py:169
  193.1 1.6 copy-start.20
  (22 other events, 18.5 us)
Sparse Core Ops, SparseCore 0:
  23.0 46.8 all-gather.1
  104.2 72.8 reduce-scatter.6
  193.2 269.0 all-reduce.2
  465.3 22.3 reduce-scatter.4
where the time goes:
time: 500 us; the launch traced here: 499 us
  waiting for transfers between devices  373 us (75%)
  local copies, waits for them, and re-layouts  54.1 us (11%)
  matrix products  40.2 us (8%)
  other arithmetic  16.9 us (3%)
  between operations  14.6 us (3%)
    psum x1, waiting for transfers between devices, body(): grad_wq, grad_wkv = lax.psum((grad_wq, grad_wkv), 'sp')  266 us
    reduce_scatter x1, waiting for transfers between devices, body(): lax.psum_scatter(partial_sums, 'sp', scatter_dimension=0, tiled=True)  51 us
    all_gather x1, waiting for transfers between devices, body(): kv_every = lax.all_gather(kv_rot, 'sp', axis=0, tiled=True)  35.3 us
    unnamed x112, local copies, waits for them, and re-layouts  26.3 us
    reduce_scatter x1, waiting for transfers between devices, body(): lax.psum_scatter(head_part.astype(jnp.bfloat16), 'dp', scatter_dimension=...  20.6 us
  transfers between devices with their start and end apart: 4, of which 4 were waited for; matrix products, arithmetic and copies ran while one was open for 8% of the time, Pallas kernels for 0%

commit v1 on v0

--- a/solution.py
+++ b/solution.py
@@ -105,7 +105,34 @@
     q_rot = rotate(q_normed * query_gain, cos_wide, sin_wide).astype(jnp.bfloat16)
     k_rot = rotate(k_normed * key_gain, cos_wide, sin_wide).astype(jnp.bfloat16)
     kv_rot = jnp.concatenate([k_rot.reshape(tok_rows, key_width), kv_raw[:, key_width:]], axis=1)
-    kv_every = lax.all_gather(kv_rot, "sp", axis=0, tiled=True)
+
+    def rest_axis_part(vals, link_axis, where_dim):
+        latest, item_now, r_now = (
+            lax.axis_size(link_axis),
+            lax.axis_index(link_axis),
+            vals.shape[where_dim],
+        )
+        part_next = jnp.zeros(
+            [i0 * latest if num == where_dim else i0 for num, i0 in enumerate(vals.shape)],
+            vals.dtype,
+        )
+        x_next = lax.dynamic_update_slice_in_dim(part_next, vals, item_now * r_now, axis=where_dim)
+        low = z2 = vals
+        for it in range(1, latest // 2 + 1):
+            low = lax.ppermute(low, link_axis, [(num, (num + 1) % latest) for num in range(latest)])
+            x_next = lax.dynamic_update_slice_in_dim(
+                x_next, low, (item_now - it) % latest * r_now, axis=where_dim
+            )
+            if 2 * it < latest:
+                z2 = lax.ppermute(
+                    z2, link_axis, [(num, (num - 1) % latest) for num in range(latest)]
+                )
+                x_next = lax.dynamic_update_slice_in_dim(
+                    x_next, z2, (item_now + it) % latest * r_now, axis=where_dim
+                )
+        return x_next
+
+    kv_every = rest_axis_part(kv_rot, "sp", 0)
     seq_rows = kv_every.shape[0]
     keys_every = kv_every[:, :key_width]
     values_every = kv_every[:, key_width:]

time: 500 us -> 518 us (1.036)
  waiting for transfers between devices: 373 us -> 342 us
  matrix products: 40.2 us -> 68.4 us
  starting transfers between devices: 0.16 us -> 18.6 us
    all_gather x1 -> x0, waiting for transfers between devices: 35.3 us -> none  [body(): kv_every = lax.all_gather(kv_rot, 'sp', axis=0, tiled=True)]
    ppermute x0 -> x7, starting transfers between devices: none -> 18.5 us  [the longest x3 11.3 us: rest_axis_part(): lax.ppermute(z2, link_axis, [(num, (num - 1) % latest) for num in range(l...]
    ppermute x0 -> x7, waiting for transfers between devices: none -> 8.64 us  [the longest x4 8.63 us: rest_axis_part(): lax.ppermute(low, link_axis, [(num, (num + 1) % latest) for num in range(...]
    dot_general x8, matrix products: 3.17 us -> 11.6 us  [body(): lax.dot_general(grad_head, value_head, contract, preferred_element_type=j...]
    dot_general x8, matrix products: 3.8 us -> 11.8 us  [body(): jnp.dot(prob_half, value_head, preferred_element_type=jnp.float32)]
    unnamed x112 -> x110, local copies, waits for them, and re-layouts: 26.3 us -> 19.4 us
    dot_general x8, matrix products: 5.09 us -> 12 us  [body(): lax.dot_general(query_head, key_head, contract, preferred_element_type=jn...]
    dynamic_update_slice x0 -> x7, local copies, waits for them, and re-layouts: none -> 6.68 us  [the longest x4 3.68 us: rest_axis_part(): lax.dynamic_update_slice_in_dim(x_next, low, (item_now - it) % latest * r...]
  transfers between devices with their start and end apart: 4 -> 10, of which waited for: 4 -> 6; matrix products, arithmetic and copies ran while one was open for 8% -> 10% of each run, Pallas kernels for 0% -> 0%
where the time goes in v1:
time: 518 us; the launch traced here: 516 us
  waiting for transfers between devices  342 us (66%)
  matrix products  68.4 us (13%)
  local copies, waits for them, and re-layouts  55.2 us (11%)
  starting transfers between devices  18.6 us (4%)
  other arithmetic  17.2 us (3%)
  between operations  14.7 us (3%)
    psum x1, waiting for transfers between devices, body(): grad_wq, grad_wkv = lax.psum((grad_wq, grad_wkv), 'sp')  266 us
    reduce_scatter x1, waiting for transfers between devices, body(): lax.psum_scatter(partial_sums, 'sp', scatter_dimension=0, tiled=True)  46.2 us
    reduce_scatter x1, waiting for transfers between devices, body(): lax.psum_scatter(head_part.astype(jnp.bfloat16), 'dp', scatter_dimension=...  20.8 us
    unnamed x110, local copies, waits for them, and re-layouts  19.4 us
    dot_general x8, matrix products, body(): jnp.dot(dscore, key_head, preferred_element_type=jnp.float32) * scale  12.3 us
    dot_general x8, matrix products, body(): lax.dot_general(query_head, key_head, contract, preferred_element_type=jn...  12 us
    dot_general x8, matrix products, body(): jnp.dot(prob_half, value_head, preferred_element_type=jnp.float32)  11.8 us
    dot_general x8, matrix products, body(): lax.dot_general(grad_head, value_head, contract, preferred_element_type=j...  11.6 us
  transfers between devices with their start and end apart: 10, of which 6 were waited for; matrix products, arithmetic and copies ran while one was open for 10% of the time, Pallas kernels for 0%

profile of v1, /device:TPU:0, one launch (start us, length us, event | category | flops | bytes accessed | tf_op | source)
XLA Modules:
  0.0 515.8 jit_solution(12537165987026961216)
XLA Ops:
  16.6 1.7 copy.97
  23.3 3.0 collective-permute-start
  26.3 3.0 collective-permute-start.1
  40.0 4.7 collective-permute-start.3
  44.7 1.6 constant_dynamic-update-slice_fusion.8
  46.3 1.6 constant_dynamic-update-slice_fusion.7
  49.3 1.7 collective-permute-start.4
  51.0 3.5 collective-permute-start.5
  55.9 2.6 collective-permute-done.4
  58.5 2.5 collective-permute-start.6
  62.4 4.6 collective-permute-done.6
  101.6 1.6 fusion.18
  106.9 1.6 fusion.24
  117.2 3.5 copy.117
  123.0 2.0 copy.109
  125.0 1.7 fusion.53
  128.3 1.6 fusion.49
  129.9 1.6 fusion.47
  138.1 1.6 multiply_reduce_fusion
  139.7 2.0 copy.106
  144.8 2.8 fusion.156
  147.5 46.2 %reduce-scatter.7.cloned.1.call-done = f32[192,512]{1,0:T(8,128)} async-done(((f32[1536,512]{1,0:T(8,128)}), f32[192,512]{1,0:T(8,128)}) %reduce-scatter.7.cloned.1.call-update) | async-done | bytes 393232 | tf_op jit(solution)/shard_map/reduce_scatter | solution.py:178
  193.7 1.6 slice.233
  195.3 1.8 copy.112
  198.2 1.6 pad_maximum_fusion
  199.8 1.8 copy.113
  202.4 1.7 copy.114
  207.1 2.7 fusion.96
  213.1 266.0 %all-reduce.3.cloned.1.call-done = (f32[512,2048]{1,0:T(8,128)}, f32[512,2048]{1,0:T(8,128)}) async-done(((f32[512,2048]{1,0:T(8,128)}, f32[512,2048]{1,0:T(8,128)}), (f32[512,2048]{1,0:T(8,128)}, f32[512,2048]{1,0:T(8,128)})) %all-reduce.3.cloned.1.call-update) | async-done | bytes 8388624 | tf_op jit(solution)/shard_map/psum | solution.py:201
  479.1 4.7 fusion.142
  483.8 20.8 %reduce-scatter.5.cloned.1.call-done = bf16[192,512]{1,0:T(8,128)(2,1)} async-done(((bf16[192,2048]{1,0:T(8,128)(2,1)}), bf16[192,512]{1,0:T(8,128)(2,1)}) %reduce-scatter.5.cloned.1.call-update) | async-done | bytes 196624 | tf_op jit(solution)/shard_map/reduce_scatter | solution.py:196
  504.5 4.7 copy.152
  (239 shorter events, 96.9 us)
Async XLA Ops:
  7.2 22.2 %copy-start = (bf16[512,2048]{1,0:T(8,128)(2,1)S(1)}, bf16[512,2048]{1,0:T(8,128)(2,1)}, u32[]{:S(2)}) copy-start(bf16[512,2048]{1,0:T(8,128)(2,1)} %param.8) | copy-start | bytes 6291460
  7.2 186.5 %reduce-scatter.7.cloned.1.call-start = ((), (), s32[]{:S(2)}) async-start(), calls=%async_computation.3 | async-start | bytes 3538944 | tf_op jit(solution)/shard_map/reduce_scatter | solution.py:178
  8.1 12.0 %copy-start.42 = (f32[256]{0:T(256)}, f32[256]{0:T(256)S(1)}, u32[]{:S(2)}) copy-start(f32[256]{0:T(256)S(1)} %mul.376) | copy-start | bytes 3076
  9.0 128.6 %copy-start.27 = (f32[192,64]{0,1:T(8,128)}, f32[192,64]{0,1:T(8,128)S(1)}, u32[]{:S(2)}) copy-start(f32[192,64]{0,1:T(8,128)S(1)} %pad_maximum_fusion.5) | copy-start | bytes 147460
  9.1 11.0 %copy-start.23 = (f32[192,256]{1,0:T(8,128)}, f32[192,256]{1,0:T(8,128)S(1)}, u32[]{:S(2)}) copy-start(f32[192,256]{1,0:T(8,128)S(1)} %copy.96) | copy-start | bytes 589828
  11.9 3.1 copy-start.47
  14.9 3.5 copy-start.20
  23.3 16.6 %collective-permute-start = (bf16[192,512]{1,0:T(8,128)(2,1)}, bf16[192,512]{1,0:T(8,128)(2,1)}, u32[]{:S(2)}, u32[]{:S(2)}) collective-permute-start(bf16[192,512]{1,0:T(8,128)(2,1)} %get-tuple-element.36), channel_id=1, source_target_pairs={{0,4},{4,8},{8,12},{12,16},{16,20},{20,24},{24,28},{28,0},{1,5},{5... | collective-permute-start | bytes 589832 | tf_op jit(solution)/shard_map/ppermute | solution.py:122
  26.3 13.7 %collective-permute-start.1 = (bf16[192,512]{1,0:T(8,128)(2,1)}, bf16[192,512]{1,0:T(8,128)(2,1)}, u32[]{:S(2)}, u32[]{:S(2)}) collective-permute-start(bf16[192,512]{1,0:T(8,128)(2,1)} %get-tuple-element.36), channel_id=1, source_target_pairs={{0,28},{4,0},{8,4},{12,8},{16,12},{20,16},{24,20},{28,24},{1,29},{... | collective-permute-start | bytes 589832 | tf_op jit(solution)/shard_map/ppermute | solution.py:127
  30.9 6.8 %copy-start.44 = (f32[64]{0:T(128)S(1)}, f32[64]{0:T(128)}, u32[]{:S(2)}) copy-start(f32[64]{0:T(128)} %param.11) | copy-start | bytes 772
  39.9 9.4 %collective-permute-start.2 = (bf16[192,512]{1,0:T(8,128)(2,1)}, bf16[192,512]{1,0:T(8,128)(2,1)S(1)}, u32[]{:S(2)}, u32[]{:S(2)}) collective-permute-start(bf16[192,512]{1,0:T(8,128)(2,1)} %collective-permute-done), channel_id=1, source_target_pairs={{0,4},{4,8},{8,12},{12,16},{16,20},{20,24},{24,28},{28,0},{1,5},{5... | collective-permute-start | bytes 589832 | tf_op jit(solution)/shard_map/ppermute | solution.py:122
  40.0 11.1 %collective-permute-start.3 = (bf16[192,512]{1,0:T(8,128)(2,1)}, bf16[192,512]{1,0:T(8,128)(2,1)S(1)}, u32[]{:S(2)}, u32[]{:S(2)}) collective-permute-start(bf16[192,512]{1,0:T(8,128)(2,1)} %collective-permute-done.1), channel_id=1, source_target_pairs={{0,28},{4,0},{8,4},{12,8},{16,12},{20,16},{24,20},{28,24},{1,29},{... | collective-permute-start | bytes 589832 | tf_op jit(solution)/shard_map/ppermute | solution.py:127
  49.3 9.2 %collective-permute-start.4 = (bf16[192,512]{1,0:T(8,128)(2,1)S(1)}, bf16[192,512]{1,0:T(8,128)(2,1)S(1)}, u32[]{:S(2)}, u32[]{:S(2)}) collective-permute-start(bf16[192,512]{1,0:T(8,128)(2,1)S(1)} %collective-permute-done.2), channel_id=1, source_target_pairs={{0,4},{4,8},{8,12},{12,16},{16,20},{20,24},{24,28},{28,0},{1,5},{5... | collective-permute-start | bytes 589832 | tf_op jit(solution)/shard_map/ppermute | solution.py:122
  51.0 10.7 %collective-permute-start.5 = (bf16[192,512]{1,0:T(8,128)(2,1)S(1)}, bf16[192,512]{1,0:T(8,128)(2,1)S(1)}, u32[]{:S(2)}, u32[]{:S(2)}) collective-permute-start(bf16[192,512]{1,0:T(8,128)(2,1)S(1)} %collective-permute-done.3), channel_id=1, source_target_pairs={{0,28},{4,0},{8,4},{12,8},{16,12},{20,16},{24,20},{28,24},{1,29},{... | collective-permute-start | bytes 589832 | tf_op jit(solution)/shard_map/ppermute | solution.py:127
  58.5 8.5 %collective-permute-start.6 = (bf16[192,512]{1,0:T(8,128)(2,1)S(1)}, bf16[192,512]{1,0:T(8,128)(2,1)S(1)}, u32[]{:S(2)}, u32[]{:S(2)}) collective-permute-start(bf16[192,512]{1,0:T(8,128)(2,1)S(1)} %collective-permute-done.4), channel_id=1, source_target_pairs={{0,4},{4,8},{8,12},{12,16},{16,20},{20,24},{24,28},{28,0},{1,5},{5... | collective-permute-start | bytes 589832 | tf_op jit(solution)/shard_map/ppermute | solution.py:122
  91.6 17.1 %copy-start.11 = (bf16[192,1536]{1,0:T(8,128)(2,1)}, bf16[192,1536]{1,0:T(8,128)(2,1)S(1)}, u32[]{:S(2)}) copy-start(bf16[192,1536]{1,0:T(8,128)(2,1)S(1)} %fusion.23) | copy-start | bytes 1769476
  95.0 14.7 %copy-start.12 = (bf16[192,1536]{1,0:T(8,128)(2,1)}, bf16[192,1536]{1,0:T(8,128)(2,1)S(1)}, u32[]{:S(2)}) copy-start(bf16[192,1536]{1,0:T(8,128)(2,1)S(1)} %fusion.21) | copy-start | bytes 1769476
  98.2 12.5 %copy-start.14 = (bf16[192,1536]{1,0:T(8,128)(2,1)}, bf16[192,1536]{1,0:T(8,128)(2,1)S(1)}, u32[]{:S(2)}) copy-start(bf16[192,1536]{1,0:T(8,128)(2,1)S(1)} %fusion.19) | copy-start | bytes 1769476
  101.6 10.1 %copy-start.16 = (bf16[192,1536]{1,0:T(8,128)(2,1)}, bf16[192,1536]{1,0:T(8,128)(2,1)S(1)}, u32[]{:S(2)}) copy-start(bf16[192,1536]{1,0:T(8,128)(2,1)S(1)} %fusion.17) | copy-start | bytes 1769476
  120.7 358.3 %all-reduce.3.cloned.1.call-start = ((), (), s32[]{:S(2)}) async-start(), calls=%async_computation.4 | async-start | bytes 16777216 | tf_op jit(solution)/shard_map/psum | solution.py:201
  125.0 3.3 copy-start.9
  126.7 3.2 copy-start.13
  128.3 3.2 copy-start.7
  129.9 3.0 copy-start.15
  132.9 3.0 copy-start.17
  139.7 3.7 copy-start.46
  147.5 50.7 %copy-start.21 = (f32[192,256]{0,1:T(8,128)S(1)}, f32[192,256]{0,1:T(8,128)}, u32[]{:S(2)}) copy-start(f32[192,256]{0,1:T(8,128)} %copy-done.20) | copy-start | bytes 589828
  147.5 50.7 %copy-start.48 = (f32[64]{0:T(128)S(1)}, f32[64]{0:T(128)}, u32[]{:S(2)}) copy-start(f32[64]{0:T(128)} %param.12) | copy-start | bytes 772
  198.2 6.9 %copy-start.24 = (f32[192,256]{1,0:T(8,128)S(1)}, f32[192,256]{1,0:T(8,128)}, u32[]{:S(2)}) copy-start(f32[192,256]{1,0:T(8,128)} %copy-done.23) | copy-start | bytes 589828
  198.2 6.9 %copy-start.43 = (f32[256]{0:T(256)S(1)}, f32[256]{0:T(256)}, u32[]{:S(2)}) copy-start(f32[256]{0:T(256)} %copy-done.42) | copy-start | bytes 3076
  199.8 5.3 %copy-start.26 = (f32[192,256]{1,0:T(8,128)S(1)}, f32[192,256]{1,0:T(8,128)}, u32[]{:S(2)}) copy-start(f32[192,256]{1,0:T(8,128)} %copy-done.25) | copy-start | bytes 589828
  209.8 294.7 %reduce-scatter.5.cloned.1.call-start = ((), (), s32[]{:S(2)}) async-start(), calls=%async_computation.2 | async-start | bytes 983040 | tf_op jit(solution)/shard_map/reduce_scatter | solution.py:196
  (27 other events, 42.6 us)
Sparse Core Ops, SparseCore 0:
  120.9 72.8 reduce-scatter.6
  209.9 269.0 all-reduce.2
  482.2 22.3 reduce-scatter.4
